TPU v7x, 32 devices: a whole 2x2x4 slice. The times are simulated.
32 devices in a mesh: ep: 4 (over y, x), tp: 8 (over z, core).
Axes of the slice: x: 2, y: 2, z: 4, core: 2. Of those that a mesh axis runs over, the one named last changes fastest.
Arguments:
- queries: bfloat16 [2048, 16, 128], P('ep', 'tp'), may hold values from -125 to 125
- keys: bfloat16 [2048, 16, 128], P('ep', 'tp'), may hold values from -9 to 9
- values: bfloat16 [2048, 16, 128], P('ep', 'tp'), may hold values from -6 to 6
- mixing: float32 [16], P('tp'), may hold values from 0.3 to 0.8
- head_gain: float32 [128], replicated, may hold values from 0.1 to 1.9
- out_weight: bfloat16 [16, 128, 2048], P('tp'), may hold values from -0.125 to 0.125
- tokens_b: bfloat16 [4096, 2048], P(('ep', 'tp')), may hold values from -6 to 6
- norm_gain: float32 [2048], replicated, may hold values from 0.1 to 1.9
- expert_ids: int32 [4096, 2], P(('ep', 'tp')), may hold values from 0 to 3, all different within a row; in each aligned block of 128 rows (0 to 127, 128 to 255, ...) at most 96 rows name the same one
- group_gate: float32 [4096], P(('ep', 'tp')), may hold values from 0.2 to 1
- expert_gate: float32 [4096, 2], P(('ep', 'tp')), may hold values from 0.1 to 0.9
- gate_weight: bfloat16 [4, 2048, 1024], P('ep', None, 'tp'), may hold values from -0.125 to 0.125
- up_weight: bfloat16 [4, 2048, 1024], P('ep', None, 'tp'), may hold values from -0.125 to 0.125
- down_weight: bfloat16 [4, 2048, 1024], P('ep', None, 'tp'), may hold values from -0.1875 to 0.1875
Outputs:
- mixed: bfloat16 [2048, 2048], P(('ep', 'tp'))
- routed: bfloat16 [4096, 2048], P(('ep', 'tp'))
Inputs may be any that keep to these rules, and one draw needn't show every extreme that they name: `expert_ids`: within each aligned block of 128 rows, no expert is named by more than 96 rows, and some block has an expert named by exactly 96 rows.
All inputs are finite; a program needn't handle non-finite values.
Results may differ from a plain program's by a relative error of at most 0.019.
Values may be sent and summed in bfloat16 or wider, within the bound.
A program may use at most 192 MiB of HBM per device.

v0:
```python
import math
import jax
import jax.numpy as jnp
from jax import lax
from jax.sharding import PartitionSpec as P

HEAD = 64


def attend_heads(queries, keys, values, mixing, head_gain):
    shard_rows = queries.shape[0]
    head_count = queries.shape[1]
    value_width = values.shape[2]
    query_start = lax.axis_index("ep") * shard_rows
    score_scale = 1.0 / math.sqrt(HEAD)
    query_pos = query_start + lax.iota(jnp.int32, shard_rows)

    def update(running, key_block, value_block, block_start):
        key_pos = block_start + lax.iota(jnp.int32, shard_rows)
        allowed = key_pos[None, :] <= query_pos[:, None]
        fresh = []
        for map_index in range(2):
            maximum, row_sum, numerator = running[3 * map_index : 3 * map_index + 3]
            offset = map_index * HEAD
            scores = (
                jnp.einsum(
                    "qhd,khd->hqk",
                    queries[:, :, offset : offset + HEAD],
                    key_block[:, :, offset : offset + HEAD],
                    preferred_element_type=jnp.float32,
                )
                * score_scale
            )
            scores = jnp.where(allowed[None], scores, -1e30)
            newmax = jnp.maximum(maximum, jnp.max(scores, axis=2))
            shrink = jnp.exp(maximum - newmax)
            weights = jnp.exp(scores - newmax[:, :, None])
            row_sum = row_sum * shrink + jnp.sum(weights, axis=2)
            numerator = numerator * shrink[:, :, None] + jnp.einsum(
                "hqk,khe->hqe",
                weights.astype(jnp.bfloat16),
                value_block,
                preferred_element_type=jnp.float32,
            )
            fresh += [newmax, row_sum, numerator]
        return tuple(fresh)

    floor_max = jnp.full((head_count, shard_rows), -1e30, jnp.float32)
    zero_sum = jnp.zeros((head_count, shard_rows), jnp.float32)
    zero_acc = jnp.zeros((head_count, shard_rows, value_width), jnp.float32)
    start_state = (floor_max, zero_sum, zero_acc, floor_max, zero_sum, zero_acc)
    running = start_state
    key_piece = lax.all_gather(keys, "ep", axis=0, tiled=True)
    value_piece = lax.all_gather(values, "ep", axis=0, tiled=True)
    blocks = key_piece.shape[0] // shard_rows
    key_blocks = key_piece.reshape(blocks, shard_rows, head_count, key_piece.shape[2])
    value_blocks = value_piece.reshape(blocks, shard_rows, head_count, value_width)

    def visit_block(state, inputs):
        key_block, value_block, block_index = inputs
        block_start = block_index * shard_rows
        state = lax.cond(
            block_start <= query_start + shard_rows - 1,
            lambda state_in: update(state_in, key_block, value_block, block_start),
            lambda state_in: state_in,
            state,
        )
        return (state, None)

    running, unused = lax.scan(
        visit_block, running, (key_blocks, value_blocks, lax.iota(jnp.int32, blocks))
    )
    state = running
    diff = state[2] / state[1][:, :, None] - mixing[:, None, None] * state[5] / state[4][:, :, None]
    normed = diff * lax.rsqrt(jnp.mean(diff * diff, axis=2, keepdims=True) + 1e-05) * head_gain
    return normed.astype(jnp.bfloat16)


def mixer_half(queries, keys, values, mixing, head_gain, out_weight):
    attended = attend_heads(queries, keys, values, mixing, head_gain)
    return lax.psum_scatter(
        jnp.einsum("hqe,hed->qd", attended, out_weight, preferred_element_type=jnp.float32).astype(
            jnp.bfloat16
        ),
        "tp",
        scatter_dimension=0,
        tiled=True,
    )


def expert_half(
    tokens_b, norm_gain, expert_ids, group_gate, expert_gate, gate_weight, up_weight, down_weight
):
    local_rows = tokens_b.shape[0]
    width = tokens_b.shape[1]
    top_count = expert_ids.shape[1]
    ep_count = lax.axis_size("ep")
    local_count = gate_weight.shape[0]
    expert_total = ep_count * local_count
    capacity = 3 * local_rows * top_count // (2 * expert_total)
    tokens_f = tokens_b.astype(jnp.float32)
    normed = (
        tokens_f
        * lax.rsqrt(jnp.mean(tokens_f * tokens_f, axis=1, keepdims=True) + 1e-06)
        * norm_gain
    ).astype(jnp.bfloat16)
    flat_ids = expert_ids.reshape(-1)
    one_hot = (flat_ids[:, None] == lax.iota(jnp.int32, expert_total)[None, :]).astype(jnp.int32)
    slot_rank = jnp.sum((jnp.cumsum(one_hot, axis=0) - one_hot) * one_hot, axis=1)
    slot_index = flat_ids * capacity + slot_rank
    owners = jnp.full((expert_total * capacity,), local_rows, jnp.int32)
    owners = owners.at[slot_index].set(lax.iota(jnp.int32, local_rows * top_count) // top_count)
    padded = jnp.concatenate([normed, jnp.zeros((1, width), jnp.bfloat16)], axis=0)
    outgoing = padded[owners].reshape(ep_count, local_count * capacity, width)
    incoming = lax.all_to_all(outgoing, "ep", split_axis=0, concat_axis=0, tiled=True)
    expert_rows = jnp.transpose(
        incoming.reshape(ep_count, local_count, capacity, width), (1, 0, 2, 3)
    )
    expert_rows = expert_rows.reshape(local_count, ep_count * capacity, width)
    piece_gate = lax.all_gather(gate_weight, "tp", axis=2, tiled=True)
    piece_up = lax.all_gather(up_weight, "tp", axis=2, tiled=True)
    piece_down = lax.all_gather(down_weight, "tp", axis=2, tiled=True)
    gate_part = jnp.einsum(
        "jrd,jdf->jrf", expert_rows, piece_gate, preferred_element_type=jnp.float32
    )
    up_part = jnp.einsum("jrd,jdf->jrf", expert_rows, piece_up, preferred_element_type=jnp.float32)
    hidden = (jax.nn.silu(gate_part) * up_part).astype(jnp.bfloat16)
    expert_out = jnp.einsum(
        "jrf,jdf->jrd", hidden, piece_down, preferred_element_type=jnp.float32
    ).astype(jnp.bfloat16)
    outbound = jnp.transpose(
        expert_out.reshape(local_count, ep_count, capacity, width), (1, 0, 2, 3)
    )
    outbound = outbound.reshape(ep_count, local_count * capacity, width)
    returned = lax.all_to_all(outbound, "ep", split_axis=0, concat_axis=0, tiled=True).reshape(
        expert_total * capacity, width
    )
    picked = returned[slot_index].reshape(local_rows, top_count, width).astype(jnp.float32)
    route_weight = group_gate[:, None] * expert_gate
    return jnp.sum(route_weight[:, :, None] * picked, axis=1).astype(jnp.bfloat16)


def per_device(
    queries,
    keys,
    values,
    mixing,
    head_gain,
    out_weight,
    tokens_b,
    norm_gain,
    expert_ids,
    group_gate,
    expert_gate,
    gate_weight,
    up_weight,
    down_weight,
):
    mixed = mixer_half(queries, keys, values, mixing, head_gain, out_weight)
    routed = expert_half(
        tokens_b,
        norm_gain,
        expert_ids,
        group_gate,
        expert_gate,
        gate_weight,
        up_weight,
        down_weight,
    )
    return (mixed, routed)


def solution(mesh):
    placed = (
        P("ep", "tp", None),
        P("ep", "tp", None),
        P("ep", "tp", None),
        P("tp"),
        P(),
        P("tp", None, None),
        P(("ep", "tp"), None),
        P(),
        P(("ep", "tp"), None),
        P(("ep", "tp")),
        P(("ep", "tp"), None),
        P("ep", None, "tp"),
        P("ep", None, "tp"),
        P("ep", None, "tp"),
    )
    return jax.shard_map(
        per_device,
        mesh=mesh,
        in_specs=placed,
        out_specs=(P(("ep", "tp"), None), P(("ep", "tp"), None)),
        check_vma=False,
    )
```

profile of v0, /device:TPU:0, one launch (start us, length us, event | category | flops | bytes accessed | tf_op | source)
XLA Modules:
  0.0 260.2 jit_solution(6079203360803837472)
XLA Ops:
  7.3 1.8 copy.24
  9.1 1.7 copy.25
  13.4 1.2 reduce-window.6
  15.3 1.4 scatter_custom_fusion
  17.0 1.0 fusion.33
  17.9 21.8 %all-gather.6.cloned.1.call-done = bf16[2048,2,128]{2,0,1:T(8,128)(2,1)} async-done(((bf16[512,2,128]{2,0,1:T(8,128)(2,1)}), bf16[2048,2,128]{2,0,1:T(8,128)(2,1)}) %all-gather.6.cloned.1.call-update) | async-done | bytes 1048592 | tf_op jit(solution)/shard_map/all_gather | solution.py:53
  39.7 2.3 copy.26
  42.0 26.1 %all-gather.8.cloned.1.call-done = bf16[2048,2,128]{2,0,1:T(8,128)(2,1)} async-done(((bf16[512,2,128]{2,0,1:T(8,128)(2,1)}), bf16[2048,2,128]{2,0,1:T(8,128)(2,1)}) %all-gather.8.cloned.1.call-update) | async-done | bytes 1048592 | tf_op jit(solution)/shard_map/all_gather | solution.py:54
  68.1 1.3 copy.28
  69.5 9.8 %while.23 = (s32[]{:T(128)}, f32[2,512]{1,0:T(2,128)S(1)}, f32[2,512]{1,0:T(2,128)S(1)}, f32[2,512,128]{2,1,0:T(8,128)S(1)}, f32[2,512]{1,0:T(2,128)S(1)}, /*ind...) while((s32[]{:T(128)}, f32[2,512]{1,0:T(2,128)S(1)}, ...), condition=%wide.region_7.8_spmd.clone, body=%wide.region_0.7_spmd.clone.sunk | while | flops 410784768 | bytes 17183128 | solution.py:70
  70.8 4.6 %conditional.3 = ((f32[2,512]{1,0:T(2,128)S(1)}, f32[2,512]{1,0:T(2,128)S(1)}, f32[2,512,128]{2,1,0:T(8,128)S(1)}, f32[2,512]{1,0:T(2,128)S(1)}, f32[2,512]{1,0:T(2,128)S(1)}, /*index=5*/f32[2,512,128]{2,1,0:T(8,128)S(1)})) conditional(s32[]{:T(128)} %convert_element_type.87, (f32[2,512]{1,0:T(2,128)S(1)}, f32[2,512]{1,0:T(2,128)S(1)}, ...), branch_computations={%region_1.1_spmd, %region_2.6_spmd} | conditional | flops 410784768 | bytes 17180748 | solution.py:62
  70.8 1.0 dynamic-slice_bitcast_fusion
  79.9 2.1 bitcast_convert_fusion
  82.2 2.5 gather_fusion
  84.6 36.1 %all_to_all.10 = bf16[4,96,2048]{2,1,0:T(8,128)(2,1)} all-to-all(bf16[4,96,2048]{2,1,0:T(8,128)(2,1)S(1)} %bitcast.62), channel_id=1, replica_groups=mesh['ep'=4,'tp'=8] {'ep'}, dimensions={0} | all-to-all | bytes 3145728 | tf_op jit(solution)/shard_map/all_to_all | solution.py:115
  120.7 5.7 %fusion.24 = f32[384,1024]{1,0:T(8,128)} fusion(bf16[384,2048]{1,0:T(8,128)(2,1)} %bitcast.63, bf16[1,2048,1024]{2,1,0:T(8,128)(2,1)} %all-gather.10.cloned.1.call-done), kind=kOutput, calls=%fused_computation.38 | convolution fusion | flops 1610612736 | bytes 7340032 | tf_op jit(solution)/shard_map/jrd,jdf->jrf/dot_general | solution.py:123
  126.4 38.6 %all-gather.12.cloned.1.call-done = bf16[1,2048,1024]{2,1,0:T(8,128)(2,1)} async-done(((bf16[1,2048,128]{2,1,0:T(8,128)(2,1)}), bf16[1,2048,1024]{2,1,0:T(8,128)(2,1)}) %all-gather.12.cloned.1.call-update) | async-done | bytes 4194320 | tf_op jit(solution)/shard_map/all_gather | solution.py:121
  165.0 47.5 %all-gather.14.cloned.1.call-done = bf16[1,2048,1024]{2,1,0:T(8,128)(2,1)} async-done(((bf16[1,2048,128]{2,1,0:T(8,128)(2,1)}), bf16[1,2048,1024]{2,1,0:T(8,128)(2,1)}) %all-gather.14.cloned.1.call-update) | async-done | bytes 4194320 | tf_op jit(solution)/shard_map/all_gather | solution.py:122
  212.5 8.6 %fusion.26 = bf16[384,2048]{1,0:T(8,128)(2,1)} fusion(bf16[1,2048,1024]{2,1,0:T(8,128)(2,1)} %all-gather.14.cloned.1.call-done, f32[384,1024]{1,0:T(8,128)} %fusion.24, bf16[384,2048]{1,0:T(8,128)(2,1)S(1)} %bitcast.64, bf16[1,2048,1024]{2,1,0:T(8,128)(2,1)} %all-gather.12.cloned.1.call-done), kind=kOutput, calls=%fused_computation.41 | convolution fusion | flops 3224371200 | bytes 13107200 | tf_op jit(solution)/shard_map/jrf,jdf->jrd/dot_general | solution.py:128
  221.1 3.8 %all-to-all-start.1 = ((bf16[4,96,2048]{2,1,0:T(8,128)(2,1)}), bf16[4,96,2048]{2,1,0:T(8,128)(2,1)S(1)}, u32[]{:S(2)}, u32[]{:S(2)}) async-start(bf16[4,96,2048]{2,1,0:T(8,128)(2,1)} %bitcast.65), calls=%async_computation.2 | async-start | bytes 3145728 | tf_op jit(solution)/shard_map/all_to_all | solution.py:135
  225.0 19.7 %all-to-all-done.1 = bf16[4,96,2048]{2,1,0:T(8,128)(2,1)S(1)} async-done(((bf16[4,96,2048]{2,1,0:T(8,128)(2,1)}), bf16[4,96,2048]{2,1,0:T(8,128)(2,1)S(1)}, u32[]{:S(2)}, u32[]{:S(2)}) %all-to-all-start.1) | async-done | bytes 1572896 | tf_op jit(solution)/shard_map/all_to_all | solution.py:135
  244.7 2.3 gather_fusion.1
  247.1 2.4 reshape.163
  249.4 3.9 %multiply_reduce_fusion = bf16[128,2048]{1,0:T(8,128)(2,1)} fusion(f32[128,2,2048]{2,1,0:T(2,128)S(1)} %reshape.163, f32[128,2]{1,0:T(8,128)S(1)} %copy.29), kind=kLoop, calls=%fused_computation.42 | loop fusion | flops 786432 | bytes 2622464 | tf_op jit(solution)/shard_map/reduce_sum | solution.py:140
  (95 shorter events, 10.3 us)
Async XLA Ops:
  7.2 72.7 %copy-start = (bf16[2,128,2048]{2,1,0:T(8,128)(2,1)S(1)}, bf16[2,128,2048]{2,1,0:T(8,128)(2,1)}, u32[]{:S(2)}) copy-start(bf16[2,128,2048]{2,1,0:T(8,128)(2,1)} %param.23) | copy-start | bytes 3145732
  7.2 5.6 %copy-start.6 = (s32[128,2]{0,1:T(2,128)S(1)}, s32[128,2]{0,1:T(2,128)}, u32[]{:S(2)}) copy-start(s32[128,2]{0,1:T(2,128)} %param.26) | copy-start | bytes 3076
  7.2 6.0 %copy-start.4 = (bf16[512,2,128]{2,1,0:T(2,128)(2,1)S(1)}, bf16[512,2,128]{2,1,0:T(2,128)(2,1)}, u32[]{:S(2)}) copy-start(bf16[512,2,128]{2,1,0:T(2,128)(2,1)} %param.18) | copy-start | bytes 786436
  7.2 9.5 %copy-start.1 = (bf16[128,2048]{1,0:T(8,128)(2,1)S(1)}, bf16[128,2048]{1,0:T(8,128)(2,1)}, u32[]{:S(2)}) copy-start(bf16[128,2048]{1,0:T(8,128)(2,1)} %param.24) | copy-start | bytes 1572868
  7.2 32.5 %all-gather.6.cloned.1.call-start = ((), (), s32[]{:S(2)}) async-start(), calls=%async_computation.3 | async-start | bytes 1310720 | tf_op jit(solution)/shard_map/all_gather | solution.py:53
  9.1 7.9 %copy-start.5 = (f32[2048]{0:T(1024)S(1)}, f32[2048]{0:T(1024)}, u32[]{:S(2)}) copy-start(f32[2048]{0:T(1024)} %param.25) | copy-start | bytes 24580
  9.1 59.0 %all-gather.8.cloned.1.call-start = ((), (), s32[]{:S(2)}) async-start(), calls=%async_computation.4 | async-start | bytes 1310720 | tf_op jit(solution)/shard_map/all_gather | solution.py:54
  10.8 109.8 %all-gather.10.cloned.1.call-start = ((), (), s32[]{:S(2)}) async-start(), calls=%async_computation.6 | async-start | bytes 4718592 | tf_op jit(solution)/shard_map/all_gather | solution.py:120
  11.6 153.4 %all-gather.12.cloned.1.call-start = ((), (), s32[]{:S(2)}) async-start(), calls=%async_computation.7 | async-start | bytes 4718592 | tf_op jit(solution)/shard_map/all_gather | solution.py:121
  12.2 200.3 %all-gather.14.cloned.1.call-start = ((), (), s32[]{:S(2)}) async-start(), calls=%async_computation.8 | async-start | bytes 4718592 | tf_op jit(solution)/shard_map/all_gather | solution.py:122
  12.7 240.6 %reduce-scatter.2.cloned.1.call-start = ((), (), s32[]{:S(2)}) async-start(), calls=%async_computation.5 | async-start | bytes 2359296 | tf_op jit(solution)/shard_map/reduce_scatter | solution.py:81
  69.5 9.9 %copy-start.8 = (f32[2]{0:T(128)S(1)}, f32[2]{0:T(128)}, u32[]{:S(2)}) copy-start(f32[2]{0:T(128)} %param.21) | copy-start | bytes 28
  69.5 10.4 %copy-start.9 = (f32[128]{0:T(128)S(1)}, f32[128]{0:T(128)}, u32[]{:S(2)}) copy-start(f32[128]{0:T(128)} %param.22) | copy-start | bytes 1540
  79.9 2.2 copy-start.2
  120.7 91.8 %copy-start.3 = (bf16[4,96,2048]{2,1,0:T(8,128)(2,1)S(1)}, bf16[4,96,2048]{2,1,0:T(8,128)(2,1)}, u32[]{:S(2)}) copy-start(bf16[4,96,2048]{2,1,0:T(8,128)(2,1)} %all_to_all.10) | copy-start | bytes 4718596
  221.1 3.8 %copy-start.7 = (f32[128,2]{0,1:T(2,128)S(1)}, f32[128,2]{0,1:T(2,128)}, u32[]{:S(2)}) copy-start(f32[128,2]{0,1:T(2,128)} %param.28) | copy-start | bytes 3076
  221.1 3.8 %copy-start.10 = (f32[128]{0:T(128)S(1)}, f32[128]{0:T(128)}, u32[]{:S(2)}) copy-start(f32[128]{0:T(128)} %param.27) | copy-start | bytes 1540
  221.1 23.6 %all-to-all-start.1 = ((bf16[4,96,2048]{2,1,0:T(8,128)(2,1)}), bf16[4,96,2048]{2,1,0:T(8,128)(2,1)S(1)}, u32[]{:S(2)}, u32[]{:S(2)}) async-start(bf16[4,96,2048]{2,1,0:T(8,128)(2,1)} %bitcast.65), calls=%async_computation.2 | async-start | bytes 3145728 | tf_op jit(solution)/shard_map/all_to_all | solution.py:135
Sparse Core Ops, SparseCore 0:
  10.4 29.2 all-gather.5
  41.5 26.4 all-gather.7
  69.7 47.8 all-gather.9
  119.0 45.9 all-gather.11
  166.4 45.9 all-gather.13
  215.2 34.1 reduce-scatter.1
where the time goes:
time: 261 us; the launch traced here: 260 us
  waiting for transfers between devices  155 us (59%)
  blocking collectives  36.1 us (14%)
  local copies, waits for them, and re-layouts  20.4 us (8%)
  matrix products  19.2 us (7%)
  between operations  14.4 us (6%)
  other arithmetic  7.89 us (3%)
  starting transfers between devices  4.02 us (2%)
  loops' own time  2.93 us (1%)
    all_gather x1, waiting for transfers between devices, expert_half(): piece_down = lax.all_gather(down_weight, 'tp', axis=2, tiled=True)  47.5 us
    all_gather x1, waiting for transfers between devices, expert_half(): piece_up = lax.all_gather(up_weight, 'tp', axis=2, tiled=True)  38.6 us
    all_to_all x1, blocking collectives, expert_half(): lax.all_to_all(outgoing, 'ep', split_axis=0, concat_axis=0, tiled=True)  36.1 us
    all_gather x1, waiting for transfers between devices, attend_heads(): value_piece = lax.all_gather(values, 'ep', axis=0, tiled=True)  26.1 us
    all_gather x1, waiting for transfers between devices, attend_heads(): key_piece = lax.all_gather(keys, 'ep', axis=0, tiled=True)  21.8 us
    all_to_all x1, waiting for transfers between devices, expert_half(): lax.all_to_all(outbound, 'ep', split_axis=0, concat_axis=0, tiled=True)  19.7 us
    dot_general x1, matrix products, expert_half(): jnp.einsum('jrf,jdf->jrd', hidden, piece_down, preferred_element_type=jnp...  8.63 us
    unnamed x28, local copies, waits for them, and re-layouts  7.42 us
  transfers between devices with their start and end apart: 7, of which 5 were waited for; matrix products, arithmetic and copies ran while one was open for 18% of the time, Pallas kernels for 0%

commit v1 on v0

--- a/solution.py
+++ b/solution.py
@@ -3,8 +3,26 @@
 import jax.numpy as jnp
 from jax import lax
 from jax.sharding import PartitionSpec as P
+from jax.lax import axis_index, axis_size, ppermute
 
 HEAD = 64
+
+
+def lay_regions(sample, out_dim, mine_x, array_axis):
+    peer_axis = "tp"
+    fields = []
+    main, t1, piece_out = (axis_size(peer_axis), axis_index(peer_axis), sample.shape[out_dim])
+    for num in range(main):
+        front = (
+            ppermute(sample, peer_axis, [(c, (c + 1) % main) for c in range(main)])
+            if num + 1 < main
+            else sample
+        )
+        fields.append(mine_x(sample, (t1 - num) % main * piece_out))
+        sample = front
+    newest = jnp.concatenate(fields[::-1], array_axis)
+    ready = jnp.roll(newest, (t1 + 1) * fields[0].shape[array_axis], array_axis)
+    return ready
 
 
 def attend_heads(queries, keys, values, mixing, head_gain):
@@ -118,12 +136,18 @@
     )
     expert_rows = expert_rows.reshape(local_count, ep_count * capacity, width)
     piece_gate = lax.all_gather(gate_weight, "tp", axis=2, tiled=True)
-    piece_up = lax.all_gather(up_weight, "tp", axis=2, tiled=True)
     piece_down = lax.all_gather(down_weight, "tp", axis=2, tiled=True)
     gate_part = jnp.einsum(
         "jrd,jdf->jrf", expert_rows, piece_gate, preferred_element_type=jnp.float32
     )
-    up_part = jnp.einsum("jrd,jdf->jrf", expert_rows, piece_up, preferred_element_type=jnp.float32)
+    up_part = lay_regions(
+        up_weight,
+        2,
+        lambda part, at: jnp.einsum(
+            "jrd,jdf->jrf", expert_rows, part, preferred_element_type=jnp.float32
+        ),
+        2,
+    )
     hidden = (jax.nn.silu(gate_part) * up_part).astype(jnp.bfloat16)
     expert_out = jnp.einsum(
         "jrf,jdf->jrd", hidden, piece_down, preferred_element_type=jnp.float32

time: 261 us -> 231 us (0.89)
  blocking collectives: 36.1 us -> 0 us
  waiting for transfers between devices: 155 us -> 140 us
  local copies, waits for them, and re-layouts: 20.4 us -> 29.8 us
  matrix products: 19.2 us -> 27 us
  starting transfers between devices: 4.02 us -> 9.23 us
    ppermute x0 -> x7, waiting for transfers between devices: none -> 60.9 us  [lay_regions(): ppermute(sample, peer_axis, [(c, (c + 1) % main) for c in range(main)])]
    all_gather x1, waiting for transfers between devices: 47.5 us -> 0.01 us  [expert_half(): piece_down = lax.all_gather(down_weight, 'tp', axis=2, tiled=True)]
    all_gather x1, waiting for transfers between devices: 0.01 us -> 45.6 us  [expert_half(): piece_gate = lax.all_gather(gate_weight, 'tp', axis=2, tiled=True)]
    all_gather x1 -> x0, waiting for transfers between devices: 38.6 us -> none  [expert_half(): piece_up = lax.all_gather(up_weight, 'tp', axis=2, tiled=True)]
    all_to_all x1 -> x0, blocking collectives: 36.1 us -> none  [expert_half(): lax.all_to_all(outgoing, 'ep', split_axis=0, concat_axis=0, tiled=True)]
    all_gather x1, waiting for transfers between devices: 21.8 us -> 0.01 us  [attend_heads(): key_piece = lax.all_gather(keys, 'ep', axis=0, tiled=True)]
    all_gather x1, waiting for transfers between devices: 26.1 us -> 12.2 us  [attend_heads(): value_piece = lax.all_gather(values, 'ep', axis=0, tiled=True)]
    dot_general x1 -> x8, matrix products: 5.74 us -> 13.5 us  [expert_half(): jnp.einsum('jrd,jdf->jrf', expert_rows, part, preferred_element_type=jnp....]
  transfers between devices with their start and end apart: 7 -> 14, of which waited for: 5 -> 9; matrix products, arithmetic and copies ran while one was open for 18% -> 27% of each run, Pallas kernels for 0% -> 0%
where the time goes in v1:
time: 231 us
  waiting for transfers between devices  140 us (61%)
  local copies, waits for them, and re-layouts  29.8 us (13%)
  matrix products  27 us (12%)
  between operations  14.1 us (6%)
  starting transfers between devices  9.23 us (4%)
  other arithmetic  8.14 us (4%)
  loops' own time  2.9 us (1%)
    ppermute x7, waiting for transfers between devices, lay_regions(): ppermute(sample, peer_axis, [(c, (c + 1) % main) for c in range(main)])  60.9 us
    all_gather x1, waiting for transfers between devices, expert_half(): piece_gate = lax.all_gather(gate_weight, 'tp', axis=2, tiled=True)  45.6 us
    all_to_all x1, waiting for transfers between devices, expert_half(): lax.all_to_all(outbound, 'ep', split_axis=0, concat_axis=0, tiled=True)  19.5 us
    unnamed x49, local copies, waits for them, and re-layouts  14.1 us
    dot_general x8, matrix products, expert_half(): jnp.einsum('jrd,jdf->jrf', expert_rows, part, preferred_element_type=jnp....  13.5 us
    all_gather x1, waiting for transfers between devices, attend_heads(): value_piece = lax.all_gather(values, 'ep', axis=0, tiled=True)  12.2 us
    dot_general x1, matrix products, expert_half(): jnp.einsum('jrf,jdf->jrd', hidden, piece_down, preferred_element_type=jnp...  8.57 us
  transfers between devices with their start and end apart: 14, of which 9 were waited for; matrix products, arithmetic and copies ran while one was open for 27% of the time, Pallas kernels for 0%

profile of v1, /device:TPU:0, one launch (start us, length us, event | category | flops | bytes accessed | tf_op | source)
XLA Modules:
  0.0 230.7 jit_solution(12971844217372385272)
XLA Ops:
  7.3 1.8 copy.32
  13.0 10.6 %collective-permute-done = bf16[1,2048,128]{2,1,0:T(8,128)(2,1)S(1)} collective-permute-done((bf16[1,2048,128]{2,1,0:T(8,128)(2,1)S(1)}, bf16[1,2048,128]{2,1,0:T(8,128)(2,1)S(1)}, u32[]{:S(2)}, u32[]{:S(2)}) %collective-permute-start) | collective-permute-done | bytes 524320 | tf_op jit(solution)/shard_map/ppermute | solution.py:17
  23.9 10.2 %collective-permute-done.1 = bf16[1,2048,128]{2,1,0:T(8,128)(2,1)S(1)} collective-permute-done((bf16[1,2048,128]{2,1,0:T(8,128)(2,1)S(1)}, bf16[1,2048,128]{2,1,0:T(8,128)(2,1)S(1)}, u32[]{:S(2)}, u32[]{:S(2)}) %collective-permute-start.1) | collective-permute-done | bytes 524320 | tf_op jit(solution)/shard_map/ppermute | solution.py:17
  36.3 8.2 %collective-permute-done.2 = bf16[1,2048,128]{2,1,0:T(8,128)(2,1)S(1)} collective-permute-done((bf16[1,2048,128]{2,1,0:T(8,128)(2,1)S(1)}, bf16[1,2048,128]{2,1,0:T(8,128)(2,1)S(1)}, u32[]{:S(2)}, u32[]{:S(2)}) %collective-permute-start.2) | collective-permute-done | bytes 524320 | tf_op jit(solution)/shard_map/ppermute | solution.py:17
  44.6 10.4 %collective-permute-done.3 = bf16[1,2048,128]{2,1,0:T(8,128)(2,1)} collective-permute-done((bf16[1,2048,128]{2,1,0:T(8,128)(2,1)S(1)}, bf16[1,2048,128]{2,1,0:T(8,128)(2,1)}, u32[]{:S(2)}, u32[]{:S(2)}) %collective-permute-start.3) | collective-permute-done | bytes 524320 | tf_op jit(solution)/shard_map/ppermute | solution.py:17
  56.4 3.1 %gather_fusion = bf16[384,2048]{1,0:T(8,128)(2,1)} fusion(bf16[129,2048]{1,0:T(8,128)(2,1)S(1)} %concatenate.9, s32[1024]{0:T(1024)S(1)} %pad_clamp_fusion.1), kind=kCustom, calls=%fused_computation | custom fusion | bytes 3147264 | tf_op jit(solution)/shard_map/gather | solution.py:132
  59.5 4.4 %all-to-all-start = ((bf16[4,96,2048]{2,1,0:T(8,128)(2,1)}), bf16[4,96,2048]{2,1,0:T(8,128)(2,1)S(1)}, u32[]{:S(2)}, u32[]{:S(2)}) async-start(bf16[4,96,2048]{2,1,0:T(8,128)(2,1)} %bitcast.145), calls=%async_computation.1 | async-start | bytes 3145728 | tf_op jit(solution)/shard_map/all_to_all | solution.py:133
  66.5 2.3 %copy.34 = bf16[4,512,2,128]{1,3,2,0:T(8,128)(2,1)} copy(bf16[4,512,2,128]{3,1,0,2:T(8,128)(2,1)} %bitcast.147) | data formatting | bytes 2097152
  68.9 12.2 %all-gather.7.cloned.1.call-done = bf16[2048,2,128]{2,0,1:T(8,128)(2,1)} async-done(((bf16[512,2,128]{2,0,1:T(8,128)(2,1)}), bf16[2048,2,128]{2,0,1:T(8,128)(2,1)}) %all-gather.7.cloned.1.call-update) | async-done | bytes 1048592 | tf_op jit(solution)/shard_map/all_gather | solution.py:72
  81.1 2.3 copy.36
  84.3 10.3 %while.23 = (s32[]{:T(128)}, f32[2,512]{1,0:T(2,128)S(1)}, f32[2,512]{1,0:T(2,128)S(1)}, f32[2,512,128]{2,1,0:T(8,128)S(1)}, f32[2,512]{1,0:T(2,128)S(1)}, /*ind...) while((s32[]{:T(128)}, f32[2,512]{1,0:T(2,128)S(1)}, ...), condition=%wide.region_7.8_spmd.clone, body=%wide.region_0.7_spmd.clone.sunk | while | flops 410784768 | bytes 25571820 | solution.py:88
  85.6 5.2 %conditional.3 = ((f32[2,512]{1,0:T(2,128)S(1)}, f32[2,512]{1,0:T(2,128)S(1)}, f32[2,512,128]{2,1,0:T(8,128)S(1)}, f32[2,512]{1,0:T(2,128)S(1)}, f32[2,512]{1,0:T(2,128)S(1)}, /*index=5*/f32[2,512,128]{2,1,0:T(8,128)})) conditional(s32[]{:T(128)} %convert_element_type.88, (f32[2,512]{1,0:T(2,128)S(1)}, f32[2,512]{1,0:T(2,128)S(1)}, ...), branch_computations={%region_1.1_spmd, %region_2.6_spmd} | conditional | flops 410784768 | bytes 25569440 | solution.py:80
  96.5 2.2 bitcast_convert_fusion
  98.7 19.7 %collective-permute-done.6 = bf16[1,2048,128]{2,1,0:T(8,128)(2,1)S(1)} collective-permute-done((bf16[1,2048,128]{2,1,0:T(8,128)(2,1)}, bf16[1,2048,128]{2,1,0:T(8,128)(2,1)S(1)}, u32[]{:S(2)}, u32[]{:S(2)}) %collective-permute-start.6) | collective-permute-done | bytes 524320 | tf_op jit(solution)/shard_map/ppermute | solution.py:17
  119.7 2.3 %constant_dynamic-update-slice_fusion.14 = (f32[1,384,2048]{2,1,0:T(8,128)}, f32[1,384,128]{2,1,0:T(8,128)S(1)}) fusion(f32[1,384,2048]{2,1,0:T(8,128)} %get-tuple-element.381, bf16[384,2048]{1,0:T(8,128)(2,1)S(1)} %bitcast.136, bf16[1,2048,128]{2,1,0:T(8,128)(2,1)} %collective-permute-done.5), kind=kOutput, calls=%fused_computation.85 | convolution fusion | flops 201326592 | bytes 2490368 | tf_op jit(solution)/shard_map/jrd,jdf->jrf/dot_general | solution.py:146
  122.0 2.4 %constant_dynamic-update-slice_fusion.13 = (f32[1,384,2048]{2,1,0:T(8,128)}, f32[1,384,128]{2,1,0:T(8,128)S(1)}) fusion(f32[1,384,2048]{2,1,0:T(8,128)} %get-tuple-element.383, bf16[384,2048]{1,0:T(8,128)(2,1)S(1)} %bitcast.137, bf16[1,2048,128]{2,1,0:T(8,128)(2,1)} %collective-permute-done.4), kind=kOutput, calls=%fused_computation.84 | convolution fusion | flops 201326592 | bytes 2490368 | tf_op jit(solution)/shard_map/jrd,jdf->jrf/dot_general | solution.py:146
  124.4 2.4 %constant_dynamic-update-slice_fusion.12 = (f32[1,384,2048]{2,1,0:T(8,128)}, f32[1,384,128]{2,1,0:T(8,128)S(1)}) fusion(f32[1,384,2048]{2,1,0:T(8,128)} %get-tuple-element.385, bf16[384,2048]{1,0:T(8,128)(2,1)S(1)} %bitcast.138, bf16[1,2048,128]{2,1,0:T(8,128)(2,1)} %collective-permute-done.3), kind=kOutput, calls=%fused_computation.83 | convolution fusion | flops 201326592 | bytes 2490368 | tf_op jit(solution)/shard_map/jrd,jdf->jrf/dot_general | solution.py:146
  137.6 45.6 %all-gather.9.cloned.1.call-done = bf16[1,2048,1024]{2,1,0:T(8,128)(2,1)} async-done(((bf16[1,2048,128]{2,1,0:T(8,128)(2,1)}), bf16[1,2048,1024]{2,1,0:T(8,128)(2,1)}) %all-gather.9.cloned.1.call-update) | async-done | bytes 4194320 | tf_op jit(solution)/shard_map/all_gather | solution.py:138
  183.3 8.6 %fusion.24 = bf16[384,2048]{1,0:T(8,128)(2,1)} fusion(bf16[1,2048,1024]{2,1,0:T(8,128)(2,1)} %all-gather.11.cloned.1.call-done, f32[1,384,2048]{2,1,0:T(8,128)} %constant_dynamic-update-slice_fusion, s32[]{:T(128)S(6)} %select_n.47, bf16[384,2048]{1,0:T(8,128)(2,1)S(1)} %bitcast.143, bf16[1,2048,1024]{2,1,0:T(8,128)(2,1)} %all-gather.9.cloned.1.call-done), kind=kOutput, calls=%fused_computation.39 | convolution fusion | flops 3224371200 | bytes 13107204 | tf_op jit(solution)/shard_map/jrf,jdf->jrd/dot_general | solution.py:152
  191.8 3.9 %all-to-all-start.1 = ((bf16[4,96,2048]{2,1,0:T(8,128)(2,1)}), bf16[4,96,2048]{2,1,0:T(8,128)(2,1)S(1)}, u32[]{:S(2)}, u32[]{:S(2)}) async-start(bf16[4,96,2048]{2,1,0:T(8,128)(2,1)} %bitcast.146), calls=%async_computation.2 | async-start | bytes 3145728 | tf_op jit(solution)/shard_map/all_to_all | solution.py:159
  195.9 19.5 %all-to-all-done.1 = bf16[4,96,2048]{2,1,0:T(8,128)(2,1)S(1)} async-done(((bf16[4,96,2048]{2,1,0:T(8,128)(2,1)}), bf16[4,96,2048]{2,1,0:T(8,128)(2,1)S(1)}, u32[]{:S(2)}, u32[]{:S(2)}) %all-to-all-start.1) | async-done | bytes 1572896 | tf_op jit(solution)/shard_map/all_to_all | solution.py:159
  215.5 2.4 %gather_fusion.1 = bf16[256,2048]{1,0:T(8,128)(2,1)} fusion(bf16[384,2048]{1,0:T(8,128)(2,1)S(1)} %bitcast.144, s32[1024]{0:T(1024)S(1)} %pad_clamp_fusion), kind=kCustom, calls=%fused_computation.1 | custom fusion | bytes 2098176 | tf_op jit(solution)/shard_map/gather | solution.py:162
  217.8 2.4 %reshape.212 = f32[128,2,2048]{2,1,0:T(2,128)S(1)} reshape(bf16[256,2048]{1,0:T(8,128)(2,1)} %gather_fusion.1) | data formatting | bytes 3145728 | tf_op jit(solution)/shard_map/convert_element_type | solution.py:162
  220.2 3.9 %multiply_reduce_fusion = bf16[128,2048]{1,0:T(8,128)(2,1)} fusion(f32[128,2,2048]{2,1,0:T(2,128)S(1)} %reshape.212, f32[128,2]{1,0:T(8,128)S(1)} %copy.37), kind=kLoop, calls=%fused_computation.40 | loop fusion | flops 786432 | bytes 2622464 | tf_op jit(solution)/shard_map/reduce_sum | solution.py:164
  (142 shorter events, 32.9 us)
Async XLA Ops:
  7.2 89.3 %copy-start = (bf16[2,128,2048]{2,1,0:T(8,128)(2,1)S(1)}, bf16[2,128,2048]{2,1,0:T(8,128)(2,1)}, u32[]{:S(2)}) copy-start(bf16[2,128,2048]{2,1,0:T(8,128)(2,1)} %param.23) | copy-start | bytes 3145732
  7.2 16.4 %copy-start.4 = (bf16[128,2048]{1,0:T(8,128)(2,1)S(1)}, bf16[128,2048]{1,0:T(8,128)(2,1)}, u32[]{:S(2)}) copy-start(bf16[128,2048]{1,0:T(8,128)(2,1)} %param.24) | copy-start | bytes 1572868
  7.2 28.8 %copy-start.15 = (f32[2048]{0:T(1024)S(1)}, f32[2048]{0:T(1024)}, u32[]{:S(2)}) copy-start(f32[2048]{0:T(1024)} %param.25) | copy-start | bytes 24580
  7.2 59.3 %all-gather.5.cloned.1.call-start = ((), (), s32[]{:S(2)}) async-start(), calls=%async_computation.3 | async-start | bytes 1310720 | tf_op jit(solution)/shard_map/all_gather | solution.py:71
  9.1 72.0 %all-gather.7.cloned.1.call-start = ((), (), s32[]{:S(2)}) async-start(), calls=%async_computation.4 | async-start | bytes 1310720 | tf_op jit(solution)/shard_map/all_gather | solution.py:72
  10.9 126.8 %all-gather.11.cloned.1.call-start = ((), (), s32[]{:S(2)}) async-start(), calls=%async_computation.7 | async-start | bytes 4718592 | tf_op jit(solution)/shard_map/all_gather | solution.py:139
  11.6 171.7 %all-gather.9.cloned.1.call-start = ((), (), s32[]{:S(2)}) async-start(), calls=%async_computation.6 | async-start | bytes 4718592 | tf_op jit(solution)/shard_map/all_gather | solution.py:138
  12.2 11.4 %collective-permute-start = (bf16[1,2048,128]{2,1,0:T(8,128)(2,1)S(1)}, bf16[1,2048,128]{2,1,0:T(8,128)(2,1)S(1)}, u32[]{:S(2)}, u32[]{:S(2)}) collective-permute-start(bf16[1,2048,128]{2,1,0:T(8,128)(2,1)S(1)} %copy-done.5), channel_id=1, source_target_pairs={{0,1},{1,2},{2,3},{3,4},{4,5},{5,6},{6,7},{7,0},{8,9},{9,10},{10,1... | collective-permute-start | bytes 1572872 | tf_op jit(solution)/shard_map/ppermute | solution.py:17
  23.6 35.9 %copy-start.7 = (bf16[1,2048,128]{2,1,0:T(8,128)(2,1)}, bf16[1,2048,128]{2,1,0:T(8,128)(2,1)S(1)}, u32[]{:S(2)}) copy-start(bf16[1,2048,128]{2,1,0:T(8,128)(2,1)S(1)} %collective-permute-done) | copy-start | bytes 1572868
  23.6 10.4 %collective-permute-start.1 = (bf16[1,2048,128]{2,1,0:T(8,128)(2,1)S(1)}, bf16[1,2048,128]{2,1,0:T(8,128)(2,1)S(1)}, u32[]{:S(2)}, u32[]{:S(2)}) collective-permute-start(bf16[1,2048,128]{2,1,0:T(8,128)(2,1)S(1)} %collective-permute-done), channel_id=1, source_target_pairs={{0,1},{1,2},{2,3},{3,4},{4,5},{5,6},{6,7},{7,0},{8,9},{9,10},{10,1... | collective-permute-start | bytes 1572872 | tf_op jit(solution)/shard_map/ppermute | solution.py:17
  34.0 25.5 %copy-start.9 = (bf16[1,2048,128]{2,1,0:T(8,128)(2,1)}, bf16[1,2048,128]{2,1,0:T(8,128)(2,1)S(1)}, u32[]{:S(2)}) copy-start(bf16[1,2048,128]{2,1,0:T(8,128)(2,1)S(1)} %collective-permute-done.1) | copy-start | bytes 1572868
  34.0 10.4 %collective-permute-start.2 = (bf16[1,2048,128]{2,1,0:T(8,128)(2,1)S(1)}, bf16[1,2048,128]{2,1,0:T(8,128)(2,1)S(1)}, u32[]{:S(2)}, u32[]{:S(2)}) collective-permute-start(bf16[1,2048,128]{2,1,0:T(8,128)(2,1)S(1)} %collective-permute-done.1), channel_id=1, source_target_pairs={{0,1},{1,2},{2,3},{3,4},{4,5},{5,6},{6,7},{7,0},{8,9},{9,10},{10,1... | collective-permute-start | bytes 1572872 | tf_op jit(solution)/shard_map/ppermute | solution.py:17
  44.5 15.1 %copy-start.11 = (bf16[1,2048,128]{2,1,0:T(8,128)(2,1)}, bf16[1,2048,128]{2,1,0:T(8,128)(2,1)S(1)}, u32[]{:S(2)}) copy-start(bf16[1,2048,128]{2,1,0:T(8,128)(2,1)S(1)} %collective-permute-done.2) | copy-start | bytes 1572868
  44.5 10.5 %collective-permute-start.3 = (bf16[1,2048,128]{2,1,0:T(8,128)(2,1)S(1)}, bf16[1,2048,128]{2,1,0:T(8,128)(2,1)}, u32[]{:S(2)}, u32[]{:S(2)}) collective-permute-start(bf16[1,2048,128]{2,1,0:T(8,128)(2,1)S(1)} %collective-permute-done.2), channel_id=1, source_target_pairs={{0,1},{1,2},{2,3},{3,4},{4,5},{5,6},{6,7},{7,0},{8,9},{9,10},{10,1... | collective-permute-start | bytes 1572872 | tf_op jit(solution)/shard_map/ppermute | solution.py:17
  55.0 10.7 %collective-permute-start.4 = (bf16[1,2048,128]{2,1,0:T(8,128)(2,1)}, bf16[1,2048,128]{2,1,0:T(8,128)(2,1)}, u32[]{:S(2)}, u32[]{:S(2)}) collective-permute-start(bf16[1,2048,128]{2,1,0:T(8,128)(2,1)} %collective-permute-done.3), channel_id=1, source_target_pairs={{0,1},{1,2},{2,3},{3,4},{4,5},{5,6},{6,7},{7,0},{8,9},{9,10},{10,1... | collective-permute-start | bytes 1572872 | tf_op jit(solution)/shard_map/ppermute | solution.py:17
  59.5 6.2 %copy-start.13 = (bf16[512,2,128]{2,1,0:T(2,128)(2,1)S(1)}, bf16[512,2,128]{2,1,0:T(2,128)(2,1)}, u32[]{:S(2)}) copy-start(bf16[512,2,128]{2,1,0:T(2,128)(2,1)} %param.18) | copy-start | bytes 786436
  59.5 39.2 %all-to-all-start = ((bf16[4,96,2048]{2,1,0:T(8,128)(2,1)}), bf16[4,96,2048]{2,1,0:T(8,128)(2,1)S(1)}, u32[]{:S(2)}, u32[]{:S(2)}) async-start(bf16[4,96,2048]{2,1,0:T(8,128)(2,1)} %bitcast.145), calls=%async_computation.1 | async-start | bytes 3145728 | tf_op jit(solution)/shard_map/all_to_all | solution.py:133
  63.9 160.3 %reduce-scatter.2.cloned.1.call-start = ((), (), s32[]{:S(2)}) async-start(), calls=%async_computation.5 | async-start | bytes 2359296 | tf_op jit(solution)/shard_map/reduce_scatter | solution.py:99
  65.7 30.5 %collective-permute-start.5 = (bf16[1,2048,128]{2,1,0:T(8,128)(2,1)}, bf16[1,2048,128]{2,1,0:T(8,128)(2,1)}, u32[]{:S(2)}, u32[]{:S(2)}) collective-permute-start(bf16[1,2048,128]{2,1,0:T(8,128)(2,1)} %collective-permute-done.4), channel_id=1, source_target_pairs={{0,1},{1,2},{2,3},{3,4},{4,5},{5,6},{6,7},{7,0},{8,9},{9,10},{10,1... | collective-permute-start | bytes 1572872 | tf_op jit(solution)/shard_map/ppermute | solution.py:17
  68.9 15.4 %copy-start.14 = (bf16[512,2,128]{0,2,1:T(8,128)(2,1)S(1)}, bf16[512,2,128]{0,2,1:T(8,128)(2,1)}, u32[]{:S(2)}) copy-start(bf16[512,2,128]{0,2,1:T(8,128)(2,1)} %copy.35) | copy-start | bytes 786436
  84.3 10.4 %copy-start.18 = (f32[2]{0:T(128)S(1)}, f32[2]{0:T(128)}, u32[]{:S(2)}) copy-start(f32[2]{0:T(128)} %param.21) | copy-start | bytes 28
  84.3 12.2 %copy-start.19 = (f32[128]{0:T(128)S(1)}, f32[128]{0:T(128)}, u32[]{:S(2)}) copy-start(f32[128]{0:T(128)} %param.22) | copy-start | bytes 1540
  96.2 22.2 %collective-permute-start.6 = (bf16[1,2048,128]{2,1,0:T(8,128)(2,1)}, bf16[1,2048,128]{2,1,0:T(8,128)(2,1)S(1)}, u32[]{:S(2)}, u32[]{:S(2)}) collective-permute-start(bf16[1,2048,128]{2,1,0:T(8,128)(2,1)} %collective-permute-done.5), channel_id=1, source_target_pairs={{0,1},{1,2},{2,3},{3,4},{4,5},{5,6},{6,7},{7,0},{8,9},{9,10},{10,1... | collective-permute-start | bytes 1572872 | tf_op jit(solution)/shard_map/ppermute | solution.py:17
  191.8 23.6 %all-to-all-start.1 = ((bf16[4,96,2048]{2,1,0:T(8,128)(2,1)}), bf16[4,96,2048]{2,1,0:T(8,128)(2,1)S(1)}, u32[]{:S(2)}, u32[]{:S(2)}) async-start(bf16[4,96,2048]{2,1,0:T(8,128)(2,1)} %bitcast.146), calls=%async_computation.2 | async-start | bytes 3145728 | tf_op jit(solution)/shard_map/all_to_all | solution.py:159
  (11 other events, 35.4 us)
Sparse Core Ops, SparseCore 0:
  10.5 29.2 all-gather.4
  42.1 38.9 all-gather.6
  82.7 53.0 all-gather.10
  137.2 45.9 all-gather.8
  186.0 34.0 reduce-scatter.1
